TPU v7x, 32 devices: a whole 2x2x4 slice. The times are simulated.
32 devices in a mesh: sp: 16 (over z, y, x), tp: 2 (over core).
Axes of the slice: x: 2, y: 2, z: 4, core: 2. Of those that a mesh axis runs over, the one named last changes fastest.
Arguments:
- resid: bfloat16 [4096, 2048], P(('sp', 'tp')), may hold values from -6 to 6
- value_in: bfloat16 [4096, 1536], P('sp', 'tp'), may hold values from -6 to 6
- gate_in: bfloat16 [4096, 1536], P('sp', 'tp'), may hold values from -8 to 8
- conv_weight: float32 [31, 1536], P(None, 'tp'), may hold values from -2.5 to 2.5
- norm_gain: float32 [1536], P('tp'), may hold values from 0.1 to 1.9
- out_weight: bfloat16 [1536, 2048], replicated, may hold values from -0.15625 to 0.15625
- ffn_gain: float32 [2048], replicated, may hold values from 0.1 to 1.9
- expert_ids: int32 [4096, 2], P(('sp', 'tp')), may hold values from 0 to 31, all different within a row; in each aligned block of 128 rows (0 to 127, 128 to 255, ...) at most 16 rows name the same one
- expert_mix: float32 [4096, 2], P(('sp', 'tp')), may hold values from 0.1 to 1
- w_gate: bfloat16 [32, 2048, 1024], P(('sp', 'tp')), may hold values from -0.125 to 0.125
- w_up: bfloat16 [32, 2048, 1024], P(('sp', 'tp')), may hold values from -0.125 to 0.125
- w_down: bfloat16 [32, 1024, 2048], P(('sp', 'tp')), may hold values from -0.1875 to 0.1875
Outputs:
- layer_out: bfloat16 [4096, 2048], P(('sp', 'tp'))
Inputs may be any that keep to these rules, and one draw needn't show every extreme that they name: `expert_ids`: each row names 2 different experts; within each aligned block of 128 rows no expert is named by more than 16 rows, a bound that some block reaches.
All inputs are finite; a program needn't handle non-finite values.
Results may differ from a plain program's by a relative error of at most 0.012.
Values may be sent and summed in bfloat16 or wider, within the bound.
A program may use at most 128 MiB of HBM per device.

v0:
```python
import functools
import jax
import jax.numpy as jnp
from jax import lax
from jax.experimental import pallas as pl
from jax.experimental.pallas import tpu as pltpu
from jax.sharding import PartitionSpec as P

MESH = pl.DeviceIdType.MESH
BF = jnp.bfloat16
F32 = jnp.float32


def layer_kernel(
    sp_count, tp_count, cap, chunks,
    resid, value_in, gate_in, taps_w, gain, ffn_gain, ids, mix, ow_h, wg_h, wu_h, wd_h, out,
    wg, wu, wd, ptok, pinfo, pack, rx, hid, ys, yr, ps, pr, acc,
    tok, info, ow, gp, wide_in, cs, cf, gf,
    w_sem, pi_sem, pt_sem, d_send, d_recv, r_send, r_recv, pp_sem,
    h_sem, c_sem, g_sem,
):
    half = sp_count // 2
    n_dev = half * tp_count
    rows, width = resid.shape
    dc = width // chunks
    slots = n_dev * cap
    me_sp = lax.axis_index("sp")
    me_tp = lax.axis_index("tp")
    local = lax.rem(me_sp, half)
    base = me_sp - local
    mine = local * tp_count + me_tp
    partner = (lax.rem(me_sp + half, sp_count), me_tp)

    def peer(i):
        n = lax.rem(mine + i, n_dev)
        return n, (base + n // tp_count, lax.rem(n, tp_count))

    weights = [
        pltpu.make_async_copy(h, v, w_sem.at[k])
        for k, (h, v) in enumerate(((ow_h, ow), (wg_h, wg), (wu_h, wu), (wd_h, wd)))
    ]
    for w in weights:
        w.start()

    barrier = pltpu.get_barrier_semaphore()

    @pl.loop(1, n_dev)
    def _(i):
        pl.semaphore_signal(barrier, inc=1, device_id=peer(i)[1], device_id_type=MESH)

    last = sp_count - 1
    has_low, has_high = me_sp > 0, me_sp < last
    lower = (jnp.maximum(me_sp - 1, 0), me_tp)
    upper = (jnp.minimum(me_sp + 1, last), me_tp)
    twin = (me_sp, 1 - me_tp)
    pl.semaphore_signal(barrier, inc=1, device_id=partner, device_id_type=MESH)

    @pl.when(has_low)
    def _():
        pl.semaphore_signal(barrier, inc=1, device_id=lower, device_id_type=MESH)

    @pl.when(has_high)
    def _():
        pl.semaphore_signal(barrier, inc=1, device_id=upper, device_id_type=MESH)

    length, local_width = value_in.shape
    taps = taps_w.shape[0]
    reach = taps // 2
    halo = (reach + 15) // 16 * 16
    gated = value_in[...].astype(F32) * jax.nn.sigmoid(gate_in[...].astype(F32))
    gp[halo : halo + length, :] = gated.astype(BF)

    @pl.when(jnp.logical_not(has_low))
    def _():
        gp[0:halo, :] = jnp.zeros((halo, local_width), BF)

    @pl.when(jnp.logical_not(has_high))
    def _():
        gp[halo + length :, :] = jnp.zeros((halo, local_width), BF)

    pl.semaphore_wait(
        barrier, n_dev + has_low.astype(jnp.int32) + has_high.astype(jnp.int32)
    )

    def remote(src, dst, send, recv, where):
        return pltpu.make_async_remote_copy(
            src_ref=src, dst_ref=dst, send_sem=send, recv_sem=recv,
            device_id=where, device_id_type=MESH,
        )

    to_low = remote(
        gp.at[halo : 2 * halo], gp.at[halo + length : 2 * halo + length], h_sem.at[0], h_sem.at[1], lower
    )
    to_high = remote(gp.at[length : length + halo], gp.at[0:halo], h_sem.at[2], h_sem.at[3], upper)

    @pl.when(has_low)
    def _():
        to_low.start()

    @pl.when(has_high)
    def _():
        to_high.start()

    gain_copy = remote(gain, gf, g_sem.at[0], g_sem.at[1], twin)
    gain_copy.start()

    experts_all = sp_count * tp_count
    expert = lax.broadcasted_iota(jnp.int32, (experts_all, rows), 0).astype(F32)
    named = ids[...].astype(F32)
    hot = [jnp.where(expert == named[k : k + 1, :], 1.0, 0.0) for k in range(2)]
    earlier = lax.broadcasted_iota(jnp.int32, (rows, rows), 0)
    later = lax.broadcasted_iota(jnp.int32, (rows, rows), 1)
    before = jnp.where(earlier < later, 1.0, 0.0).astype(BF)
    rank = jnp.dot((hot[0] + hot[1]).astype(BF), before, preferred_element_type=F32)
    info[2:4, :] = mix[...]
    info[4:, :] = jnp.zeros_like(info[4:, :])
    for k in range(2):
        info[k : k + 1, :] = named[k : k + 1, :] * cap + jnp.sum(
            hot[k] * rank, axis=0, keepdims=True
        )
    info_copy = remote(info, pinfo, pi_sem.at[0], pi_sem.at[1], partner)
    info_copy.start()

    @pl.when(has_low)
    def _():
        to_high.wait_recv()

    @pl.when(has_high)
    def _():
        to_low.wait_recv()

    wide_in[...] = gp[...].astype(F32)
    span = rows + 2 * halo

    def convolve(first, put):
        @pl.loop(0, local_width // 128)
        def _(b):
            cols = pl.ds(pl.multiple_of(b * 128, 128), 128)
            x = wide_in[pl.ds(first, span), cols]
            total = jnp.zeros((rows, 128), F32)
            for r in range(8):
                offsets = [j for j in range(taps) if (j + halo - reach) % 8 == r]
                if not offsets:
                    continue
                shifted = x if r == 0 else pltpu.roll(x, span - r, 0)
                for j in offsets:
                    at = j + halo - reach - r
                    total = total + shifted[at : at + rows] * taps_w[j : j + 1, cols]
            put(cols, total)

    def put_out(cols, total):
        cs[:, cols] = total

    def put_own(cols, total):
        cf[0, :, cols] = total

    convolve(pl.multiple_of((1 - me_tp) * rows, rows), put_out)
    conv_copy = remote(cs, cf.at[1], c_sem.at[0], c_sem.at[1], twin)
    conv_copy.start()
    convolve(pl.multiple_of(me_tp * rows, rows), put_own)
    weights[0].wait()
    gain_copy.wait_recv()
    conv_copy.wait_recv()
    channels = local_width * tp_count
    mean = (jnp.sum(cf[0], axis=1, keepdims=True) + jnp.sum(cf[1], axis=1, keepdims=True)) / channels
    msq = (
        jnp.sum(cf[0] * cf[0], axis=1, keepdims=True) + jnp.sum(cf[1] * cf[1], axis=1, keepdims=True)
    ) / channels
    scale = lax.rsqrt(msq - mean * mean + 1e-05)

    def silu(v):
        return v * jax.nn.sigmoid(v)

    mixed = [
        silu((cf[0] - mean) * scale * gain[...].reshape(1, local_width)).astype(BF),
        silu((cf[1] - mean) * scale * gf[...].reshape(1, local_width)).astype(BF),
    ]
    whose = (me_tp, 1 - me_tp)
    square = jnp.zeros((rows, 1), F32)
    step = 512
    for c in range(width // step):
        cols = slice(c * step, (c + 1) * step)
        proj = jnp.zeros((rows, step), F32)
        for m, w in zip(mixed, whose):
            at = pl.ds(pl.multiple_of(w * local_width, local_width), local_width)
            proj = proj + jnp.dot(m, ow[at, cols], preferred_element_type=F32)
        wide = (resid[:, cols].astype(F32) + proj).astype(BF).astype(F32)
        acc[:, cols] = wide
        square = square + jnp.sum(wide * wide, axis=1, keepdims=True)
    rms = lax.rsqrt(square / width + 1e-06)
    for c in range(chunks):
        tok[c] = (
            acc[:, c * dc : (c + 1) * dc] * rms * ffn_gain[:, c * dc : (c + 1) * dc]
        ).astype(BF)

    quarter = sp_count // 4
    inner = (me_sp >= quarter) & (me_sp < sp_count - quarter)
    tok_copies = [
        remote(tok.at[c], ptok.at[c], pt_sem.at[0, c], pt_sem.at[1, c], partner)
        for c in range(chunks)
    ]

    @pl.when(inner)
    def _():
        for t in tok_copies:
            t.start()

    def slot_match(ref):
        ids = lax.broadcasted_iota(jnp.int32, (slots, rows), 0) + base * (tp_count * cap)
        ids = ids.astype(F32)
        return ids == ref[0:1, :], ids == ref[1:2, :]

    def exchange(src, dst, send, recv, s, c):
        @pl.loop(1, n_dev)
        def _(i):
            n, where = peer(i)
            remote(src.at[s, c, n], dst.at[s, c, mine], send.at[s, c], recv.at[s, c], where).start()

        pltpu.make_async_copy(src.at[s, c, mine], dst.at[s, c, mine], recv.at[s, c]).start()

    def all_in(dst, recv, s, c):
        pltpu.make_async_copy(dst.at[s, c], dst.at[s, c], recv.at[s, c]).wait()

    def all_out(src, send, s, c):
        part = src.at[s, c, pl.ds(0, n_dev - 1)]
        pltpu.make_async_copy(part, part, send.at[s, c]).wait()

    def pack_send(s, c, match, block):
        picked = jnp.dot(match, block, preferred_element_type=F32)
        pack[s, c] = picked.astype(BF).reshape(n_dev, cap, dc)
        exchange(pack, rx, d_send, d_recv, s, c)

    def one_hot(ref):
        a, b = slot_match(ref)
        return jnp.where(a | b, 1.0, 0.0).astype(BF)

    own = one_hot(info)
    for c in range(chunks):
        pack_send(0, c, own, tok[c])

    @pl.when(jnp.logical_not(inner))
    def _():
        for t in tok_copies:
            t.start()

    info_copy.wait_recv()
    other = one_hot(pinfo)

    def run_experts(s):
        for c in range(chunks):
            all_in(rx, d_recv, s, c)
        ff = wg.shape[1]
        tile = min(256, ff)

        @pl.loop(0, ff // tile)
        def _(f):
            cols = pl.ds(pl.multiple_of(f * tile, tile), tile)
            gate = jnp.zeros((slots, tile), F32)
            up = jnp.zeros((slots, tile), F32)
            for c in range(chunks):
                x = rx[s, c].reshape(slots, dc)
                gate = gate + jnp.dot(x, wg[c * dc : (c + 1) * dc, cols], preferred_element_type=F32)
                up = up + jnp.dot(x, wu[c * dc : (c + 1) * dc, cols], preferred_element_type=F32)
            hid[:, cols] = (gate * jax.nn.sigmoid(gate) * up).astype(BF)

        for c in range(chunks):
            y = jnp.dot(hid[...], wd[:, c * dc : (c + 1) * dc], preferred_element_type=F32)
            ys[s, c] = y.astype(BF).reshape(n_dev, cap, dc)
            if s == 1:
                exchange(ys, yr, r_send, r_recv, s, c)

    early = chunks // 2
    for c in range(early):
        tok_copies[c].wait_recv()
        pack_send(1, c, other, ptok[c])
    for w in weights[1:]:
        w.wait()
    run_experts(0)
    for c in range(early, chunks):
        tok_copies[c].wait_recv()
        pack_send(1, c, other, ptok[c])
    for c in range(early):
        exchange(ys, yr, r_send, r_recv, 0, c)
    run_experts(1)
    for c in range(early, chunks):
        exchange(ys, yr, r_send, r_recv, 0, c)

    def mix_matrix(ref):
        a, b = slot_match(ref)
        full = jnp.where(a, ref[2:3, :], 0.0) + jnp.where(b, ref[3:4, :], 0.0)
        high = full.astype(BF)
        return high, (full - high.astype(F32)).astype(BF)

    def combine(s, c, mats):
        y = yr[s, c].reshape(slots, dc)
        dims = (((0,), (0,)), ((), ()))
        return sum(lax.dot_general(m, y, dims, preferred_element_type=F32) for m in mats)

    other_mix = mix_matrix(pinfo)
    parts = []
    for c in range(chunks):
        all_in(yr, r_recv, 1, c)
        ps[c] = combine(1, c, other_mix).astype(BF)
        copy = remote(ps.at[c], pr.at[c], pp_sem.at[0, c], pp_sem.at[1, c], partner)
        copy.start()
        parts.append(copy)
    own_mix = mix_matrix(info)
    for c in range(chunks):
        all_in(yr, r_recv, 0, c)
        acc[:, c * dc : (c + 1) * dc] += combine(0, c, own_mix)
    for c in range(chunks):
        parts[c].wait_recv()
        out[:, c * dc : (c + 1) * dc] = (acc[:, c * dc : (c + 1) * dc] + pr[c].astype(F32)).astype(BF)
    info_copy.wait_send()
    gain_copy.wait_send()
    conv_copy.wait_send()

    @pl.when(has_low)
    def _():
        to_low.wait_send()

    @pl.when(has_high)
    def _():
        to_high.wait_send()

    for c in range(chunks):
        tok_copies[c].wait_send()
        parts[c].wait_send()
        for s in range(2):
            all_out(pack, d_send, s, c)
            all_out(ys, r_send, s, c)


def layer_call(resid, value_in, gate_in, taps_w, gain, ffn_gain, ids, mix, ow, w_gate, w_up, w_down, cap):
    sp_count, tp_count = lax.axis_size("sp"), lax.axis_size("tp")
    chunks = 4
    rows, width = resid.shape
    length, local_width = value_in.shape
    halo = (taps_w.shape[0] // 2 + 15) // 16 * 16
    n_dev = sp_count // 2 * tp_count
    dc = width // chunks
    ff = w_gate.shape[1]
    vm = pl.BlockSpec(memory_space=pltpu.VMEM)
    hb = pl.BlockSpec(memory_space=pl.ANY)
    blocks = pltpu.VMEM((2, chunks, n_dev, cap, dc), BF)
    dma = pltpu.SemaphoreType.DMA
    return pl.pallas_call(
        functools.partial(layer_kernel, sp_count, tp_count, cap, chunks),
        out_shape=jax.ShapeDtypeStruct((rows, width), BF),
        in_specs=[vm] * 8 + [hb] * 4,
        out_specs=vm,
        scratch_shapes=[
            pltpu.VMEM((width, ff), BF),
            pltpu.VMEM((width, ff), BF),
            pltpu.VMEM((ff, width), BF),
            pltpu.VMEM((chunks, rows, dc), BF),
            pltpu.VMEM((8, rows), F32),
            blocks,
            blocks,
            pltpu.VMEM((n_dev * cap, ff), BF),
            blocks,
            blocks,
            pltpu.VMEM((chunks, rows, dc), BF),
            pltpu.VMEM((chunks, rows, dc), BF),
            pltpu.VMEM((rows, width), F32),
            pltpu.VMEM((chunks, rows, dc), BF),
            pltpu.VMEM((8, rows), F32),
            pltpu.VMEM(ow.shape, BF),
            pltpu.VMEM((length + 2 * halo, local_width), BF),
            pltpu.VMEM((length + 2 * halo, local_width), F32),
            pltpu.VMEM((rows, local_width), F32),
            pltpu.VMEM((2, rows, local_width), F32),
            pltpu.VMEM(gain.shape, F32),
            dma((4,)),
            dma((2,)),
            dma((2, chunks)),
            dma((2, chunks)),
            dma((2, chunks)),
            dma((2, chunks)),
            dma((2, chunks)),
            dma((2, chunks)),
            dma((4,)),
            dma((2,)),
            dma((2,)),
        ],
        compiler_params=pltpu.CompilerParams(
            collective_id=0, has_side_effects=True, vmem_limit_bytes=58 * 1024 * 1024
        ),
        name="layer",
    )(resid, value_in, gate_in, taps_w, gain, ffn_gain, ids, mix, ow, w_gate, w_up, w_down)


def per_device(
    resid,
    value_in,
    gate_in,
    conv_weight,
    norm_gain,
    out_weight,
    ffn_gain,
    expert_ids,
    expert_mix,
    w_gate,
    w_up,
    w_down,
):
    experts_all = lax.axis_size("sp") * lax.axis_size("tp")
    rows_here = resid.shape[0]
    topk = expert_ids.shape[1]
    cap = max(2, (2 * topk * rows_here + experts_all - 1) // experts_all)
    return layer_call(
        resid, value_in, gate_in, conv_weight, norm_gain, ffn_gain[None], expert_ids.T, expert_mix.T,
        out_weight, w_gate[0], w_up[0], w_down[0], cap,
    )


def solution(mesh):
    return jax.shard_map(
        per_device,
        mesh=mesh,
        in_specs=(
            P(("sp", "tp"), None),
            P("sp", "tp"),
            P("sp", "tp"),
            P(None, "tp"),
            P("tp"),
            P(),
            P(),
            P(("sp", "tp"), None),
            P(("sp", "tp"), None),
            P(("sp", "tp"), None, None),
            P(("sp", "tp"), None, None),
            P(("sp", "tp"), None, None),
        ),
        out_specs=P(("sp", "tp"), None),
        check_vma=False,
    )
```

profile of v0, /device:TPU:0, one launch (start us, length us, event | category | flops | bytes accessed | tf_op | source)
XLA Modules:
  0.0 88.4 jit_solution(10485840765606040127)
XLA Ops:
  0.0 86.5 %layer.1 = bf16[128,2048]{1,0:T(8,128)(2,1)} custom-call(bf16[128,2048]{1,0:T(8,128)(2,1)} %resid.1, bf16[256,768]{1,0:T(8,128)(2,1)} %value_in.1, bf16[256,768]{1,0:T(8,128)(2,1)} %gate_in.1, f32[31,768]{1,0:T(8,128)} %taps_w.1, f32[768]{0:T(1024)} %gain.1, f32[1,2048]{1,0:T(1,128)} %bitcast.9, s32[2,128]{1,0:T(2,128)} %bitcast.10, f32[2,128]{1,0:T(2,128)} %bitcast.11, ...), custom_call_target="tpu_custom_call" | custom-call | tf_op jit(solution)/shard_map/layer/pallas_call | solution.py:347
  86.5 1.9 %copy.14 = bf16[128,2048]{1,0:T(8,128)(2,1)} copy(bf16[128,2048]{1,0:T(8,128)(2,1)} %layer.1) | data formatting | bytes 1048576
where the time goes:
time: 88.6 us; the launch traced here: 88.4 us
  Pallas kernels  86.5 us (98%)
  local copies, waits for them, and re-layouts  1.88 us (2%)
    pallas_call x1, Pallas kernels, layer_call(): pl.pallas_call(functools.partial(layer_kernel, sp_count, tp_count, cap, c...  86.5 us
    unnamed x1, local copies, waits for them, and re-layouts  1.88 us

commit v1 on v0

v1 whole, which is shorter than its diff:
```python
import functools
import jax
import jax.numpy as jnp
from jax import lax
from jax.experimental import pallas as pl
from jax.experimental.pallas import tpu as pltpu
from jax.sharding import PartitionSpec as P

MESH = pl.DeviceIdType.MESH
BF = jnp.bfloat16
F32 = jnp.float32


PLANES = 4


def layer_kernel(
    sp_count, tp_count, cap, chunks,
    resid, value_in, gate_in, taps_w, gain, ffn_gain, ids, mix, ow_h, wg_h, wu_h, wd_h, out,
    wg, wu, wd, tok, infos, pack, rx, hid, gates, ups, ys, yr, part, sums, back, acc,
    hots, mixes, ow, gp, wide_in, cs, cf, gf,
    w_sem, i_send, i_recv, t_send, t_recv, d_send, d_recv, r_send, r_recv, b_send, b_recv,
    h_sem, c_sem, g_sem,
):
    plane = sp_count // PLANES
    n_dev = plane * tp_count
    rows, width = resid.shape
    dc = width // chunks
    slots = n_dev * cap
    me_sp = lax.axis_index("sp")
    me_tp = lax.axis_index("tp")
    local = lax.rem(me_sp, plane)
    base = me_sp - local
    mine = local * tp_count + me_tp
    level = me_sp // plane
    low_half = level < PLANES // 2
    step_in = jnp.where(low_half, plane, -plane)
    is_end = (level == 0) | (level == PLANES - 1)
    is_mid = jnp.logical_not(is_end)
    inner = (me_sp + step_in, me_tp)
    outer = (jnp.where(is_mid, me_sp - step_in, me_sp), me_tp)

    def column(i):
        return (lax.rem(me_sp + i * plane, sp_count), me_tp)

    def peer(i):
        n = lax.rem(mine + i, n_dev)
        return n, (base + n // tp_count, lax.rem(n, tp_count))

    weights = [
        pltpu.make_async_copy(h, v, w_sem.at[k])
        for k, (h, v) in enumerate(((ow_h, ow), (wg_h, wg), (wu_h, wu), (wd_h, wd)))
    ]
    for w in weights:
        w.start()

    barrier = pltpu.get_barrier_semaphore()

    @pl.loop(1, n_dev)
    def _(i):
        pl.semaphore_signal(barrier, inc=1, device_id=peer(i)[1], device_id_type=MESH)

    @pl.loop(1, PLANES)
    def _(i):
        pl.semaphore_signal(barrier, inc=1, device_id=column(i), device_id_type=MESH)

    last = sp_count - 1
    has_low, has_high = me_sp > 0, me_sp < last
    lower = (jnp.maximum(me_sp - 1, 0), me_tp)
    upper = (jnp.minimum(me_sp + 1, last), me_tp)
    twin = (me_sp, 1 - me_tp)

    @pl.when(has_low)
    def _():
        pl.semaphore_signal(barrier, inc=1, device_id=lower, device_id_type=MESH)

    @pl.when(has_high)
    def _():
        pl.semaphore_signal(barrier, inc=1, device_id=upper, device_id_type=MESH)

    length, local_width = value_in.shape
    taps = taps_w.shape[0]
    reach = taps // 2
    halo = (reach + 15) // 16 * 16
    half = rows // 2
    span = half + 2 * halo
    gated = (value_in[...].astype(F32) * jax.nn.sigmoid(gate_in[...].astype(F32))).astype(BF)
    gp[halo : halo + length, :] = gated
    wide_in[halo : halo + length, :] = gated.astype(F32)

    @pl.when(jnp.logical_not(has_low))
    def _():
        gp[0:halo, :] = jnp.zeros((halo, local_width), BF)

    @pl.when(jnp.logical_not(has_high))
    def _():
        gp[halo + length :, :] = jnp.zeros((halo, local_width), BF)

    def begins(h, core):
        return pl.multiple_of(half + half * core if h == 0 else (length - half) * core, half)

    def inside(h, core):
        return pl.ds(pl.multiple_of(half * (1 - core) if h == 0 else half * core, half), half)

    def convolve(h, core, put):
        first = begins(h, core)

        @pl.loop(0, local_width // 128)
        def _(b):
            cols = pl.ds(pl.multiple_of(b * 128, 128), 128)
            x = wide_in[pl.ds(first, span), cols]
            total = jnp.zeros((half, 128), F32)
            for r in range(8):
                offsets = [j for j in range(taps) if (j + halo - reach) % 8 == r]
                if not offsets:
                    continue
                shifted = x if r == 0 else pltpu.roll(x, span - r, 0)
                for j in offsets:
                    at = j + halo - reach - r
                    total = total + shifted[at : at + half] * taps_w[j : j + 1, cols]
            put(cols, total)

    def both(h):
        def put_out(cols, total):
            cs[h, :, cols] = total

        def put_own(cols, total):
            cf[0, inside(h, me_tp), cols] = total

        return put_out, put_own

    convolve(0, 1 - me_tp, both(0)[0])
    convolve(0, me_tp, both(0)[1])

    pl.semaphore_wait(
        barrier,
        n_dev - 1 + PLANES - 1 + has_low.astype(jnp.int32) + has_high.astype(jnp.int32),
    )

    def remote(src, dst, send, recv, where):
        return pltpu.make_async_remote_copy(
            src_ref=src, dst_ref=dst, send_sem=send, recv_sem=recv,
            device_id=where, device_id_type=MESH,
        )

    to_low = remote(
        gp.at[halo : 2 * halo], gp.at[halo + length : 2 * halo + length], h_sem.at[0], h_sem.at[1], lower
    )
    to_high = remote(gp.at[length : length + halo], gp.at[0:halo], h_sem.at[2], h_sem.at[3], upper)

    @pl.when(has_low)
    def _():
        to_low.start()

    @pl.when(has_high)
    def _():
        to_high.start()

    def conv_copy(h):
        there = inside(h, 1 - me_tp)
        return remote(cs.at[h], cf.at[1, there], c_sem.at[0, h], c_sem.at[1, h], twin)

    conv_copy(0).start()
    gain_copy = remote(gain, gf, g_sem.at[0], g_sem.at[1], twin)
    gain_copy.start()

    experts_all = sp_count * tp_count
    expert = lax.broadcasted_iota(jnp.int32, (experts_all, rows), 0).astype(F32)
    named = ids[...].astype(F32)
    hot = [jnp.where(expert == named[k : k + 1, :], 1.0, 0.0) for k in range(2)]
    earlier = lax.broadcasted_iota(jnp.int32, (rows, rows), 0)
    later = lax.broadcasted_iota(jnp.int32, (rows, rows), 1)
    before = jnp.where(earlier < later, 1.0, 0.0).astype(BF)
    rank = jnp.dot((hot[0] + hot[1]).astype(BF), before, preferred_element_type=F32)
    infos[0, 2:4, :] = mix[...]
    infos[0, 4:, :] = jnp.zeros((4, rows), F32)
    for k in range(2):
        infos[0, k : k + 1, :] = named[k : k + 1, :] * cap + jnp.sum(
            hot[k] * rank, axis=0, keepdims=True
        )

    def place(there):
        at_end = (there == 0) | (there == PLANES - 1)
        gap = jnp.abs(there - level)
        return jnp.where(at_end, gap, jnp.where(is_end, jnp.where(gap == 1, 1, 3), 2))

    info_copies = []
    for i in range(1, PLANES):
        there = lax.rem(level + i, PLANES)
        info_copies.append(
            remote(infos.at[0], infos.at[place(there)], i_send.at[i], i_recv.at[place(there)], column(i))
        )
    for copy in info_copies:
        copy.start()

    channels = local_width * tp_count
    whose = (me_tp, 1 - me_tp)
    step = 512

    def silu(v):
        return v * jax.nn.sigmoid(v)

    def hop(q, src, k, c, where):
        return remote(tok.at[src, c], tok.at[k, c], t_send.at[q, c], t_recv.at[k, c], where)

    def hop_part(q, k, c, where, at):
        return remote(tok.at[0, c, at], tok.at[k, c, at], t_send.at[q, c], t_recv.at[k, c], where)

    def tokens(h):
        here = inside(h, me_tp)
        remote(cs.at[h], cf.at[1, here], c_sem.at[0, h], c_sem.at[1, h], twin).wait_recv()
        conv = [cf[i, here, :] for i in range(2)]
        mean = sum(jnp.sum(v, axis=1, keepdims=True) for v in conv) / channels
        msq = sum(jnp.sum(v * v, axis=1, keepdims=True) for v in conv) / channels
        scale = lax.rsqrt(msq - mean * mean + 1e-05)
        mixed = [
            silu((v - mean) * scale * g[...].reshape(1, local_width)).astype(BF)
            for v, g in zip(conv, (gain, gf))
        ]
        square = jnp.zeros((half, 1), F32)
        for c in range(width // step):
            cols = slice(c * step, (c + 1) * step)
            proj = jnp.zeros((half, step), F32)
            for m, w in zip(mixed, whose):
                at = pl.ds(pl.multiple_of(w * local_width, local_width), local_width)
                proj = proj + jnp.dot(m, ow[at, cols], preferred_element_type=F32)
            wide = (resid[here, cols].astype(F32) + proj).astype(BF).astype(F32)
            acc[here, cols] = wide
            square = square + jnp.sum(wide * wide, axis=1, keepdims=True)
        rms = lax.rsqrt(square / width + 1e-06)
        for c in range(chunks):
            at = slice(c * dc, (c + 1) * dc)
            tok[0, c, here, :] = (acc[here, at] * rms * ffn_gain[:, at]).astype(BF)

            @pl.when(is_mid)
            def _():
                hop_part(0, 2, c, inner, here).start()
                hop_part(1, 1, c, outer, here).start()

            @pl.when(is_end)
            def _():
                hop_part(0, 1, c, inner, here).start()

    weights[0].wait()
    gain_copy.wait_recv()
    tokens(0)

    @pl.when(has_low)
    def _():
        to_high.wait_recv()

    @pl.when(has_high)
    def _():
        to_low.wait_recv()

    wide_in[0:halo, :] = gp[0:halo, :].astype(F32)
    wide_in[halo + length :, :] = gp[halo + length :, :].astype(F32)
    convolve(1, 1 - me_tp, both(1)[0])
    conv_copy(1).start()
    convolve(1, me_tp, both(1)[1])
    tokens(1)

    def slot_match(ref):
        ids = lax.broadcasted_iota(jnp.int32, (slots, rows), 0) + base * (tp_count * cap)
        ids = ids.astype(F32)
        return ids == ref[0:1, :], ids == ref[1:2, :]

    def tables(k):
        a, b = slot_match(infos.at[k])
        hots[k] = jnp.where(a | b, 1.0, 0.0).astype(BF)
        full = jnp.where(a, infos[k, 2:3, :], 0.0) + jnp.where(b, infos[k, 3:4, :], 0.0)
        full = jnp.transpose(full)
        high = full.astype(BF)
        mixes[k, :, :slots] = high
        mixes[k, :, slots:] = (full - high.astype(F32)).astype(BF)

    few = n_dev <= 8
    peers = [peer(i) for i in range(1, n_dev)] if few else []

    def exchange(src, dst, send, recv, k, c):
        def start(n, where):
            remote(src.at[k, c, n], dst.at[k, c, mine], send.at[k, c], recv.at[k, c], where).start()

        if few:
            for n, where in peers:
                start(n, where)
        else:

            @pl.loop(1, n_dev)
            def _(i):
                start(*peer(i))

        dst[k, c, mine] = src[k, c, mine]

    def all_in(dst, recv, k, c):
        share = dst.at[k, c, pl.ds(0, n_dev - 1)]
        pltpu.make_async_copy(share, share, recv.at[k, c]).wait()

    def all_out(src, send, k, c):
        share = src.at[k, c, pl.ds(0, n_dev - 1)]
        pltpu.make_async_copy(share, share, send.at[k, c]).wait()

    def dispatch(k, c):
        picked = jnp.dot(hots[k], tok[k, c], preferred_element_type=F32)
        pack[k, c] = picked.astype(BF).reshape(n_dev, cap, dc)
        exchange(pack, rx, d_send, d_recv, k, c)

    def arrived(k, c):
        hop(0, k, k, c, inner).wait_recv()

    ff = wg.shape[1]
    tile = min(256, ff)
    pairs = chunks // 2

    def hidden(*ks):
        for k in ks:
            for c in range(chunks):
                all_in(rx, d_recv, k, c)
        n = len(ks) * slots

        @pl.loop(0, ff // tile)
        def _(f):
            cols = pl.ds(pl.multiple_of(f * tile, tile), tile)
            gate = jnp.zeros((n, tile), F32)
            up = jnp.zeros((n, tile), F32)
            for c in range(chunks):
                x = [rx[k, c].reshape(slots, dc) for k in ks]
                x = x[0] if len(ks) == 1 else jnp.concatenate(x, axis=0)
                at = slice(c * dc, (c + 1) * dc)
                gate = gate + jnp.dot(x, wg[at, cols], preferred_element_type=F32)
                up = up + jnp.dot(x, wu[at, cols], preferred_element_type=F32)
            made = (gate * jax.nn.sigmoid(gate) * up).astype(BF)
            for i, k in enumerate(ks):
                hid[k, :, cols] = made[i * slots : (i + 1) * slots]

    def hidden_part(k, j):
        for c in (2 * j, 2 * j + 1):
            all_in(rx, d_recv, k, c)

        @pl.loop(0, ff // tile)
        def _(f):
            cols = pl.ds(pl.multiple_of(f * tile, tile), tile)
            gate = up = None
            for c in (2 * j, 2 * j + 1):
                x = rx[k, c].reshape(slots, dc)
                at = slice(c * dc, (c + 1) * dc)
                g = jnp.dot(x, wg[at, cols], preferred_element_type=F32)
                u = jnp.dot(x, wu[at, cols], preferred_element_type=F32)
                gate, up = (g, u) if gate is None else (gate + g, up + u)
            if j > 0:
                gate, up = gate + gates[:, cols], up + ups[:, cols]
            if j < pairs - 1:
                gates[:, cols] = gate
                ups[:, cols] = up
            else:
                hid[k, :, cols] = (gate * jax.nn.sigmoid(gate) * up).astype(BF)

    def answer(k, c):
        exchange(ys, yr, r_send, r_recv, k, c)

    def down(ks, first, last, send=()):
        for c in range(first, last):
            x = [hid[k] for k in ks]
            x = x[0] if len(ks) == 1 else jnp.concatenate(x, axis=0)
            y = jnp.dot(x, wd[:, c * dc : (c + 1) * dc], preferred_element_type=F32).astype(BF)
            for i, k in enumerate(ks):
                ys[k, c] = y[i * slots : (i + 1) * slots].reshape(n_dev, cap, dc)
                if k in send:
                    answer(k, c)

    def combine(k, c):
        all_in(yr, r_recv, k, c)
        y = yr[k, c].reshape(slots, dc)
        return jnp.dot(mixes[k], jnp.concatenate([y, y], axis=0), preferred_element_type=F32)

    def homeward(q, slot, c, where):
        return remote(sums.at[q, c], back.at[slot, c], b_send.at[q, c], b_recv.at[slot, c], where)

    def returned(slot, c):
        homeward(0, slot, c, inner).wait_recv()
        return back[slot, c].astype(F32)

    def send_home(q, slot, c, where, value):
        sums[q, c] = value.astype(BF)
        homeward(q, slot, c, where).start()

    def add(c, value):
        acc[:, c * dc : (c + 1) * dc] += value

    tables(0)
    for c in range(chunks):
        dispatch(0, c)
    for k in range(1, PLANES):
        remote(infos.at[0], infos.at[k], i_send.at[k], i_recv.at[k], inner).wait_recv()
        tables(k)

    def take(k, *cs):
        for c in cs:
            arrived(k, c)
            dispatch(k, c)

    for w in weights[1:]:
        w.wait()
    every = range(chunks)

    @pl.when(is_end)
    def _():
        def own(*cs):
            for c in cs:
                add(c, combine(0, c))

        def home(k, *cs):
            for c in cs:
                send_home(k - 1, k - 1, c, inner, combine(k, c))

        take(1, 0, 1, 2, 3)
        hidden(0)
        down((0,), 0, 2)
        take(1, 4, 5)
        down((0,), 2, 8)
        take(1, 6, 7)
        take(2, 0, 1)
        hidden(1)
        take(2, 2)
        down((1,), 0, 3, send=(1,))
        take(2, 3)
        down((1,), 3, 8, send=(1,))
        take(2, 4, 5)
        home(1, 0, 1)
        take(2, 6)
        home(1, 2)
        take(2, 7)
        home(1, 3, 4)
        take(3, 0)
        home(1, 5, 6)
        take(3, 1)
        home(1, 7)
        take(3, 2, 3)
        hidden(2)
        down((2,), 0, 1, send=(2,))
        take(3, 4)
        hidden_part(3, 0)
        down((2,), 1, 2, send=(2,))
        hidden_part(3, 1)
        take(3, 5)
        down((2,), 2, 5, send=(2,))
        take(3, 6)
        down((2,), 5, 8, send=(2,))
        home(2, 0)
        take(3, 7)
        home(2, 1, 2)
        hidden_part(3, 2)
        home(2, 3, 4, 5, 6, 7)
        hidden_part(3, 3)
        down((3,), 0, 8, send=(3,))
        for c in every:
            answer(0, c)
        home(3, *every)
        own(*every)
        for c in every:
            at = slice(c * dc, (c + 1) * dc)
            out[:, at] = (acc[:, at] + returned(0, c)).astype(BF)
        for c in range(chunks):
            hop(0, 0, 1, c, inner).wait_send()

    @pl.when(is_mid)
    def _():
        def near(*cs):
            for c in cs:
                arrived(1, c)
                hop(2, 1, 3, c, inner).start()
                dispatch(1, c)
                arrived(2, c)
                hop(3, 2, 2, c, outer).start()
                dispatch(2, c)

        def far(*cs):
            for c in cs:
                arrived(3, c)
                hop(4, 3, 3, c, outer).start()
                dispatch(3, c)

        def keep(k, *cs):
            for c in cs:
                part[k - 1, c] = combine(k, c)

        def pass_on(q, k, slot, got, where, c):
            send_home(q, slot, c, where, part[k - 1, c] + returned(got, c))

        def finish(*cs):
            for c in cs:
                at = slice(c * dc, (c + 1) * dc)
                value = combine(0, c) + returned(0, c) + returned(3, c)
                out[:, at] = (acc[:, at] + value).astype(BF)

        def middle(c):
            pass_on(0, 2, 3, 1, inner, c)

        def onward(c):
            pass_on(1, 3, 4, 2, inner, c)

        near(0, 1, 2, 3)
        hidden(0)
        down((0,), 0, 2)
        near(4, 5)
        down((0,), 2, 8)
        near(6, 7)
        far(0, 1, 2, 3)
        hidden(1, 2)
        down((1, 2), 0, 1, send=(1,))
        far(4)
        down((1, 2), 1, 3, send=(1,))
        far(5)
        down((1, 2), 3, 5, send=(1,))
        far(6)
        down((1, 2), 5, 7, send=(1,))
        keep(1, 0)
        far(7)
        down((1, 2), 7, 8, send=(1,))
        for c in every:
            answer(2, c)
        keep(1, 1, 2, 3, 4, 5, 6)
        hidden(3)
        keep(1, 7)
        keep(2, 0)
        down((3,), 0, 2, send=(3,))
        keep(2, 1)
        down((3,), 2, 5, send=(3,))
        keep(2, 2)
        down((3,), 5, 8, send=(3,))
        for c in every:
            answer(0, c)
        keep(2, 3, 4, 5, 6)
        middle(0)
        keep(2, 7)
        keep(3, 0)
        middle(1)
        keep(3, 1, 2)
        middle(2)
        keep(3, 3, 4)
        middle(3)
        keep(3, 5, 6)
        middle(4)
        keep(3, 7)
        finish(0)
        middle(5)
        finish(1, 2)
        middle(6)
        finish(3, 4)
        middle(7)
        finish(5)
        onward(0)
        finish(6)
        onward(1)
        finish(7)
        for c in range(2, chunks + 2):
            if c < chunks:
                pass_on(1, 3, 4, 2, inner, c)
            pass_on(2, 1, 0, 4, outer, c - 2)
        for c in range(chunks):
            hop(0, 0, 2, c, inner).wait_send()
            hop(1, 0, 1, c, outer).wait_send()
            hop(2, 1, 3, c, inner).wait_send()
            hop(3, 2, 2, c, outer).wait_send()
            hop(4, 3, 3, c, outer).wait_send()

    for copy in info_copies:
        copy.wait_send()
    gain_copy.wait_send()
    conv_copy(0).wait_send()
    conv_copy(1).wait_send()

    @pl.when(has_low)
    def _():
        to_low.wait_send()

    @pl.when(has_high)
    def _():
        to_high.wait_send()

    for c in range(chunks):
        for q in range(3):
            homeward(q, q, c, inner).wait_send()
        for k in range(PLANES):
            all_out(pack, d_send, k, c)
            all_out(ys, r_send, k, c)


def layer_call(resid, value_in, gate_in, taps_w, gain, ffn_gain, ids, mix, ow, w_gate, w_up, w_down, cap):
    sp_count, tp_count = lax.axis_size("sp"), lax.axis_size("tp")
    chunks = 8
    rows, width = resid.shape
    length, local_width = value_in.shape
    halo = (taps_w.shape[0] // 2 + 15) // 16 * 16
    n_dev = sp_count // PLANES * tp_count
    dc = width // chunks
    ff = w_gate.shape[1]
    vm = pl.BlockSpec(memory_space=pltpu.VMEM)
    hb = pl.BlockSpec(memory_space=pl.ANY)
    slots = n_dev * cap
    blocks = pltpu.VMEM((PLANES, chunks, n_dev, cap, dc), BF)
    table = pltpu.VMEM((PLANES, slots, rows), BF)
    dma = pltpu.SemaphoreType.DMA
    return pl.pallas_call(
        functools.partial(layer_kernel, sp_count, tp_count, cap, chunks),
        out_shape=jax.ShapeDtypeStruct((rows, width), BF),
        in_specs=[vm] * 8 + [hb] * 4,
        out_specs=vm,
        scratch_shapes=[
            pltpu.VMEM((width, ff), BF),
            pltpu.VMEM((width, ff), BF),
            pltpu.VMEM((ff, width), BF),
            pltpu.VMEM((PLANES, chunks, rows, dc), BF),
            pltpu.VMEM((PLANES, 8, rows), F32),
            blocks,
            blocks,
            pltpu.VMEM((PLANES, slots, ff), BF),
            pltpu.VMEM((slots, ff), F32),
            pltpu.VMEM((slots, ff), F32),
            blocks,
            blocks,
            pltpu.VMEM((3, chunks, rows, dc), F32),
            pltpu.VMEM((3, chunks, rows, dc), BF),
            pltpu.VMEM((5, chunks, rows, dc), BF),
            pltpu.VMEM((rows, width), F32),
            table,
            pltpu.VMEM((PLANES, rows, 2 * slots), BF),
            pltpu.VMEM(ow.shape, BF),
            pltpu.VMEM((length + 2 * halo, local_width), BF),
            pltpu.VMEM((length + 2 * halo, local_width), F32),
            pltpu.VMEM((2, rows // 2, local_width), F32),
            pltpu.VMEM((2, rows, local_width), F32),
            pltpu.VMEM(gain.shape, F32),
            dma((4,)),
            dma((PLANES,)),
            dma((PLANES,)),
            dma((5, chunks)),
            dma((PLANES, chunks)),
            dma((PLANES, chunks)),
            dma((PLANES, chunks)),
            dma((PLANES, chunks)),
            dma((PLANES, chunks)),
            dma((3, chunks)),
            dma((5, chunks)),
            dma((4,)),
            dma((2, 2)),
            dma((2,)),
        ],
        compiler_params=pltpu.CompilerParams(
            collective_id=0, has_side_effects=True, vmem_limit_bytes=58 * 1024 * 1024
        ),
        name="layer",
    )(resid, value_in, gate_in, taps_w, gain, ffn_gain, ids, mix, ow, w_gate, w_up, w_down)


def per_device(
    resid,
    value_in,
    gate_in,
    conv_weight,
    norm_gain,
    out_weight,
    ffn_gain,
    expert_ids,
    expert_mix,
    w_gate,
    w_up,
    w_down,
):
    experts_all = lax.axis_size("sp") * lax.axis_size("tp")
    rows_here = resid.shape[0]
    topk = expert_ids.shape[1]
    cap = max(2, (2 * topk * rows_here + experts_all - 1) // experts_all)
    return layer_call(
        resid, value_in, gate_in, conv_weight, norm_gain, ffn_gain[None], expert_ids.T, expert_mix.T,
        out_weight, w_gate[0], w_up[0], w_down[0], cap,
    )


def solution(mesh):
    return jax.shard_map(
        per_device,
        mesh=mesh,
        in_specs=(
            P(("sp", "tp"), None),
            P("sp", "tp"),
            P("sp", "tp"),
            P(None, "tp"),
            P("tp"),
            P(),
            P(),
            P(("sp", "tp"), None),
            P(("sp", "tp"), None),
            P(("sp", "tp"), None, None),
            P(("sp", "tp"), None, None),
            P(("sp", "tp"), None, None),
        ),
        out_specs=P(("sp", "tp"), None),
        check_vma=False,
    )
```

time: 88.6 us -> 88.3 us (level)
  no operation moved by 1% of the time
where the time goes in v1:
time: 88.3 us; the launch traced here: 88.1 us
  Pallas kernels  86.3 us (98%)
  local copies, waits for them, and re-layouts  1.88 us (2%)
    pallas_call x1, Pallas kernels, layer_call(): pl.pallas_call(functools.partial(layer_kernel, sp_count, tp_count, cap, c...  86.3 us
    unnamed x1, local copies, waits for them, and re-layouts  1.88 us

profile of v1, /device:TPU:0, one launch (start us, length us, event | category | flops | bytes accessed | tf_op | source)
XLA Modules:
  0.0 88.1 jit_solution(15589407859715956172)
XLA Ops:
  0.0 86.3 %layer.1 = bf16[128,2048]{1,0:T(8,128)(2,1)} custom-call(bf16[128,2048]{1,0:T(8,128)(2,1)} %resid.1, bf16[256,768]{1,0:T(8,128)(2,1)} %value_in.1, bf16[256,768]{1,0:T(8,128)(2,1)} %gate_in.1, f32[31,768]{1,0:T(8,128)} %taps_w.1, f32[768]{0:T(1024)} %gain.1, f32[1,2048]{1,0:T(1,128)} %bitcast.9, s32[2,128]{1,0:T(2,128)} %bitcast.10, f32[2,128]{1,0:T(2,128)} %bitcast.11, ...), custom_call_target="tpu_custom_call" | custom-call | tf_op jit(solution)/shard_map/layer/pallas_call | solution.py:604
  86.3 1.9 %copy.14 = bf16[128,2048]{1,0:T(8,128)(2,1)} copy(bf16[128,2048]{1,0:T(8,128)(2,1)} %layer.1) | data formatting | bytes 1048576

commit v2 on v1

--- a/solution.py
+++ b/solution.py
@@ -358,8 +358,12 @@
     def answer(k, c):
         exchange(ys, yr, r_send, r_recv, k, c)
 
-    def down(ks, first, last, send=()):
-        for c in range(first, last):
+    def reply(k, *cs):
+        for c in cs:
+            answer(k, c)
+
+    def down(ks, cs, send=()):
+        for c in cs:
             x = [hid[k] for k in ks]
             x = x[0] if len(ks) == 1 else jnp.concatenate(x, axis=0)
             y = jnp.dot(x, wd[:, c * dc : (c + 1) * dc], preferred_element_type=F32).astype(BF)
@@ -409,57 +413,103 @@
             for c in cs:
                 add(c, combine(0, c))
 
+        def out_of(*cs):
+            for c in cs:
+                at = slice(c * dc, (c + 1) * dc)
+                out[:, at] = (acc[:, at] + returned(0, c)).astype(BF)
+
         def home(k, *cs):
             for c in cs:
                 send_home(k - 1, k - 1, c, inner, combine(k, c))
 
-        take(1, 0, 1, 2, 3)
+        take(1, 2, 0, 1)
         hidden(0)
-        down((0,), 0, 2)
-        take(1, 4, 5)
-        down((0,), 2, 8)
-        take(1, 6, 7)
-        take(2, 0, 1)
+        take(1, 4)
+        down((0,), (4,))
+        reply(0, 4)
+        take(1, 5, 6)
+        down((0,), (0,))
+        take(1, 7, 3)
+        take(2, 1, 0, 2, 4)
         hidden(1)
-        take(2, 2)
-        down((1,), 0, 3, send=(1,))
+        down((1,), (1,), send=(1,))
         take(2, 3)
-        down((1,), 3, 8, send=(1,))
-        take(2, 4, 5)
-        home(1, 0, 1)
-        take(2, 6)
+        down((1,), (0,), send=(1,))
+        take(2, 6, 5, 7)
+        down((1,), (4,), send=(1,))
+        down((0,), (7,))
+        take(3, 2)
+        home(1, 1, 0)
+        down((1,), (3, 7), send=(1,))
+        take(3, 3)
+        hidden(2)
+        take(3, 0)
+        down((0,), (5,))
+        down((2,), (0,), send=(2,))
+        home(1, 3)
+        take(3, 1)
+        down((0,), (2,))
+        down((2,), (1,), send=(2,))
+        home(1, 4)
+        down((2,), (6,), send=(2,))
+        take(3, 4)
+        down((2,), (4,), send=(2,))
+        home(1, 7)
+        take(3, 7, 5)
+        home(2, 0)
+        hidden_part(3, 0)
+        take(3, 6)
+        down((2,), (3,), send=(2,))
+        home(2, 1)
+        reply(0, 2)
+        home(2, 6)
+        down((2,), (2,), send=(2,))
+        home(2, 4)
+        hidden_part(3, 1)
+        hidden_part(3, 2)
+        reply(0, 0)
+        hidden_part(3, 3)
+        down((3,), (2,), send=(3,))
+        home(2, 3)
+        down((3,), (7, 4), send=(3,))
+        down((2,), (5,), send=(2,))
+        down((3,), (5,), send=(3,))
+        home(2, 2)
+        down((3,), (1,), send=(3,))
+        own(4)
+        reply(0, 7)
+        down((3,), (6,), send=(3,))
+        home(3, 2)
+        down((3,), (0,), send=(3,))
+        home(3, 7)
+        own(2)
+        home(3, 4)
+        down((3,), (3,), send=(3,))
+        down((1,), (6,), send=(1,))
+        home(3, 1)
+        down((1,), (2,), send=(1,))
+        down((0,), (6,))
+        down((2,), (7,), send=(2,))
+        own(7)
+        home(3, 5, 3, 6, 0)
+        down((0,), (1, 3))
+        reply(0, 5)
+        home(1, 6)
+        reply(0, 3)
         home(1, 2)
-        take(2, 7)
-        home(1, 3, 4)
-        take(3, 0)
-        home(1, 5, 6)
-        take(3, 1)
-        home(1, 7)
-        take(3, 2, 3)
-        hidden(2)
-        down((2,), 0, 1, send=(2,))
-        take(3, 4)
-        hidden_part(3, 0)
-        down((2,), 1, 2, send=(2,))
-        hidden_part(3, 1)
-        take(3, 5)
-        down((2,), 2, 5, send=(2,))
-        take(3, 6)
-        down((2,), 5, 8, send=(2,))
-        home(2, 0)
-        take(3, 7)
-        home(2, 1, 2)
-        hidden_part(3, 2)
-        home(2, 3, 4, 5, 6, 7)
-        hidden_part(3, 3)
-        down((3,), 0, 8, send=(3,))
-        for c in every:
-            answer(0, c)
-        home(3, *every)
-        own(*every)
-        for c in every:
-            at = slice(c * dc, (c + 1) * dc)
-            out[:, at] = (acc[:, at] + returned(0, c)).astype(BF)
+        reply(0, 1)
+        down((1,), (5,), send=(1,))
+        reply(0, 6)
+        home(2, 5, 7)
+        own(1)
+        out_of(1)
+        own(6)
+        out_of(2)
+        home(1, 5)
+        own(3)
+        out_of(3, 4, 6)
+        own(0, 5)
+        out_of(5, 7, 0)
         for c in range(chunks):
             hop(0, 0, 1, c, inner).wait_send()
 
@@ -493,70 +543,109 @@
                 value = combine(0, c) + returned(0, c) + returned(3, c)
                 out[:, at] = (acc[:, at] + value).astype(BF)
 
-        def middle(c):
-            pass_on(0, 2, 3, 1, inner, c)
-
-        def onward(c):
-            pass_on(1, 3, 4, 2, inner, c)
-
-        near(0, 1, 2, 3)
+        def middle(*cs):
+            for c in cs:
+                pass_on(0, 2, 3, 1, inner, c)
+
+        def onward(*cs):
+            for c in cs:
+                pass_on(1, 3, 4, 2, inner, c)
+
+        def late(*cs):
+            for c in cs:
+                pass_on(2, 1, 0, 4, outer, c)
+
+        near(4, 0, 1, 2, 3)
         hidden(0)
-        down((0,), 0, 2)
-        near(4, 5)
-        down((0,), 2, 8)
+        near(5)
+        down((0,), (7, 1))
         near(6, 7)
-        far(0, 1, 2, 3)
+        far(2, 3, 0)
         hidden(1, 2)
-        down((1, 2), 0, 1, send=(1,))
+        down((1, 2), (7,), send=(1,))
+        far(1)
+        reply(0, 7)
         far(4)
-        down((1, 2), 1, 3, send=(1,))
-        far(5)
-        down((1, 2), 3, 5, send=(1,))
-        far(6)
-        down((1, 2), 5, 7, send=(1,))
+        down((0,), (6,))
+        down((1, 2), (5,), send=(1,))
+        reply(2, 7)
+        down((0,), (3,))
+        down((1, 2), (4, 0), send=(1,))
+        far(7, 5, 6)
+        down((0,), (2,))
+        reply(2, 0)
+        down((1, 2), (3, 1), send=(1,))
+        down((0,), (0,))
+        down((1, 2), (6,), send=(1,))
+        reply(2, 4)
+        reply(0, 3)
+        keep(1, 7)
+        hidden(3)
+        down((1, 2), (2,), send=(1,))
+        keep(2, 0)
+        reply(0, 0)
+        down((3,), (2,), send=(3,))
+        reply(2, 6)
+        down((3,), (5,), send=(3,))
+        down((0,), (5,))
+        down((3,), (1,), send=(3,))
+        reply(2, 1, 2)
+        down((3,), (0,), send=(3,))
+        keep(1, 2)
+        middle(0)
+        down((3,), (4,), send=(3,))
+        keep(2, 6, 4)
+        middle(6)
+        down((3,), (3, 7), send=(3,))
+        keep(1, 5)
+        down((3,), (6,), send=(3,))
+        reply(2, 5)
+        middle(4)
+        keep(2, 1)
+        middle(1)
+        reply(0, 6)
+        keep(1, 1)
+        keep(3, 1, 0)
+        keep(1, 4)
+        reply(2, 3)
+        keep(3, 4)
+        keep(1, 3)
+        keep(3, 2)
+        onward(2)
+        keep(3, 7)
+        onward(7)
+        keep(1, 6)
+        onward(4, 1)
+        keep(3, 5)
+        late(2)
+        keep(2, 7)
+        keep(3, 6, 3)
+        keep(2, 3)
+        onward(5)
+        late(7)
+        down((0,), (4,))
+        onward(3)
+        reply(0, 4)
+        late(4)
+        onward(6)
         keep(1, 0)
-        far(7)
-        down((1, 2), 7, 8, send=(1,))
-        for c in every:
-            answer(2, c)
-        keep(1, 1, 2, 3, 4, 5, 6)
-        hidden(3)
-        keep(1, 7)
-        keep(2, 0)
-        down((3,), 0, 2, send=(3,))
-        keep(2, 1)
-        down((3,), 2, 5, send=(3,))
+        late(1)
+        onward(0)
+        reply(0, 1)
+        late(5)
+        reply(0, 2)
         keep(2, 2)
-        down((3,), 5, 8, send=(3,))
-        for c in every:
-            answer(0, c)
-        keep(2, 3, 4, 5, 6)
-        middle(0)
-        keep(2, 7)
-        keep(3, 0)
-        middle(1)
-        keep(3, 1, 2)
+        middle(3)
+        late(3)
+        reply(0, 5)
+        keep(2, 5)
         middle(2)
-        keep(3, 3, 4)
-        middle(3)
-        keep(3, 5, 6)
-        middle(4)
-        keep(3, 7)
-        finish(0)
+        late(6)
+        finish(6)
         middle(5)
-        finish(1, 2)
-        middle(6)
-        finish(3, 4)
+        late(0)
         middle(7)
-        finish(5)
-        onward(0)
-        finish(6)
-        onward(1)
-        finish(7)
-        for c in range(2, chunks + 2):
-            if c < chunks:
-                pass_on(1, 3, 4, 2, inner, c)
-            pass_on(2, 1, 0, 4, outer, c - 2)
+        finish(4, 2, 1, 0, 3, 5, 7)
         for c in range(chunks):
             hop(0, 0, 2, c, inner).wait_send()
             hop(1, 0, 1, c, outer).wait_send()

time: 88.3 us -> 84 us (0.951)
  Pallas kernels: 86.3 us -> 81.9 us
    pallas_call x1, Pallas kernels: 86.3 us -> 81.9 us  [layer_call(): pl.pallas_call(functools.partial(layer_kernel, sp_count, tp_count, cap, c...]
where the time goes in v2:
time: 84 us; the launch traced here: 83.8 us
  Pallas kernels  81.9 us (98%)
  local copies, waits for them, and re-layouts  1.88 us (2%)
    pallas_call x1, Pallas kernels, layer_call(): pl.pallas_call(functools.partial(layer_kernel, sp_count, tp_count, cap, c...  81.9 us
    unnamed x1, local copies, waits for them, and re-layouts  1.88 us

profile of v2, /device:TPU:0, one launch (start us, length us, event | category | flops | bytes accessed | tf_op | source)
XLA Modules:
  0.0 83.8 jit_solution(7494506294462087888)
XLA Ops:
  0.0 81.9 %layer.1 = bf16[128,2048]{1,0:T(8,128)(2,1)} custom-call(bf16[128,2048]{1,0:T(8,128)(2,1)} %resid.1, bf16[256,768]{1,0:T(8,128)(2,1)} %value_in.1, bf16[256,768]{1,0:T(8,128)(2,1)} %gate_in.1, f32[31,768]{1,0:T(8,128)} %taps_w.1, f32[768]{0:T(1024)} %gain.1, f32[1,2048]{1,0:T(1,128)} %bitcast.9, s32[2,128]{1,0:T(2,128)} %bitcast.10, f32[2,128]{1,0:T(2,128)} %bitcast.11, ...), custom_call_target="tpu_custom_call" | custom-call | tf_op jit(solution)/shard_map/layer/pallas_call | solution.py:693
  81.9 1.9 %copy.14 = bf16[128,2048]{1,0:T(8,128)(2,1)} copy(bf16[128,2048]{1,0:T(8,128)(2,1)} %layer.1) | data formatting | bytes 1048576
